TPU v7x, 32 devices: a whole 2x2x4 slice. The times are simulated.
32 devices in a mesh: sp: 8 (over z, x), tp: 4 (over y, core).
Axes of the slice: x: 2, y: 2, z: 4, core: 2. Of those that a mesh axis runs over, the one named last changes fastest.
Arguments:
- residual: bfloat16 [4096, 2048], P(('sp', 'tp')), may hold values from -6 to 6
- conv_value: bfloat16 [4096, 1024], P('sp', 'tp'), may hold values from -6 to 6
- conv_gate: bfloat16 [4096, 1024], P('sp', 'tp'), may hold values from -9 to 9
- segments: int32 [4096], P('sp'), may hold values from 0 to 3, never falling along the last dimension, each value on 1 to 2048 neighbouring positions
- conv_weight: float32 [31, 1024], P(None, 'tp'), may hold values from -1 to 1
- norm_gain: float32 [1024], P('tp'), may hold values from 0.1 to 1.9
- norm_shift: float32 [1024], P('tp'), may hold values from -3 to 3
- out_weight: bfloat16 [1024, 2048], replicated, may hold values from -0.1875 to 0.1875
- ffn_gain: float32 [2048], replicated, may hold values from 0.1 to 1.9
- routes: int32 [4096, 2], P('sp'), may hold values from 0 to 7, all different within a row; in each aligned block of 128 rows (0 to 127, 128 to 255, ...) at most 64 rows name the same one
- route_weights: float32 [4096, 2], P('sp'), may hold values from 0.2 to 1
- w_gate: bfloat16 [8, 2048, 1024], P('sp', None, 'tp'), may hold values from -0.125 to 0.125
- w_up: bfloat16 [8, 2048, 1024], P('sp', None, 'tp'), may hold values from -0.125 to 0.125
- w_down: bfloat16 [8, 1024, 2048], P('sp', 'tp'), may hold values from -0.1875 to 0.1875
Outputs:
- layer_out: bfloat16 [4096, 2048], P(('sp', 'tp'))
Inputs may be any that keep to these rules, and one draw needn't show every extreme that they name: `routes`: within the rows of one device (aligned blocks of 512 / 4 rows), no expert is named more than 64 times; the two experts of a row differ. `segments`: document numbers never fall along the sequence.
All inputs are finite; a program needn't handle non-finite values.
Results may differ from a plain program's by a relative error of at most 0.007.
Values may be sent and summed in bfloat16 or wider, within the bound.
A program may use at most 128 MiB of HBM per device.

v0:
```python
import jax
import jax.numpy as jnp
from jax import lax
from jax.sharding import PartitionSpec as P

DC = 1024
CONV_GROUPS = 8


def passed_along(value, axis, steps):
    count = lax.axis_size(axis)
    initial, last = (max(0, -steps), min(count, count - steps))
    return lax.ppermute(value, axis, [(source, source + steps) for source in range(initial, last)])


def slot_numbers(block_routes, capacity, experts_n):
    route_pairs = block_routes.reshape(block_routes.shape[:-2] + (-1,))
    onehot = (route_pairs[..., None] == jnp.arange(experts_n, dtype=jnp.int32)).astype(jnp.int32)
    slot_rank = jnp.sum((jnp.cumsum(onehot, axis=-2) - onehot) * onehot, axis=-1)
    return (route_pairs * capacity + slot_rank).reshape(block_routes.shape)


def dispatch_matrix(slot_ids, slot_total):
    numbers = jnp.arange(slot_total, dtype=jnp.int32)[:, None, None]
    matches = jnp.any(numbers == slot_ids[..., None, :, :], axis=-1)
    return matches.astype(jnp.bfloat16)


def shards(
    residual,
    conv_value,
    conv_gate,
    segments,
    conv_weight,
    norm_gain,
    norm_shift,
    out_weight,
    ffn_gain,
    routes,
    route_weights,
    w_gate,
    w_up,
    w_down,
):
    tok_dev, local_channels = conv_value.shape
    reach = conv_weight.shape[0] - 1
    whole_gate, whole_up = (
        lax.all_gather(w_gate[0], "tp", axis=1, tiled=True),
        lax.all_gather(w_up[0], "tp", axis=1, tiled=True),
    )
    whole_down = lax.all_gather(w_down[0], "tp", axis=0, tiled=True)
    gated = (conv_value.astype(jnp.float32) * jax.nn.sigmoid(conv_gate.astype(jnp.float32))).astype(
        jnp.bfloat16
    )
    rim_prev, seg_prev = passed_along(
        (gated[tok_dev - reach :], segments[tok_dev - reach :]), "sp", 1
    )
    extended = jnp.concatenate([rim_prev, gated], 0).astype(jnp.float32)
    seg_ext = jnp.concatenate([seg_prev, segments], 0)
    convolved = jnp.zeros((tok_dev, local_channels), jnp.float32)
    for offset in range(reach + 1):
        same_doc = (seg_ext[offset : offset + tok_dev] == segments)[:, None]
        convolved = convolved + jnp.where(
            same_doc, extended[offset : offset + tok_dev] * conv_weight[offset], 0.0
        )
    group_size = DC // CONV_GROUPS
    grouped = convolved.reshape(tok_dev, local_channels // group_size, group_size)
    group_mean = jnp.mean(grouped, axis=-1, keepdims=True)
    group_var = jnp.mean(jnp.square(grouped - group_mean), axis=-1, keepdims=True)
    scaled = ((grouped - group_mean) * lax.rsqrt(group_var + 1e-05)).reshape(
        tok_dev, local_channels
    ) * norm_gain + norm_shift
    conv_out = jax.nn.silu(scaled).astype(jnp.bfloat16)
    columns = lax.axis_size("tp")
    column = lax.axis_index("tp")
    rows_own = tok_dev // columns
    own_conv = lax.all_to_all(conv_out, "tp", split_axis=0, concat_axis=1, tiled=True)
    mixed = jnp.dot(own_conv, out_weight, preferred_element_type=jnp.float32)
    stream = residual.astype(jnp.float32) + lax.optimization_barrier(
        mixed.astype(jnp.bfloat16)
    ).astype(jnp.float32)
    normed = (
        stream * lax.rsqrt(jnp.mean(stream * stream, axis=-1, keepdims=True) + 1e-06) * ffn_gain
    ).astype(jnp.bfloat16)
    experts_n = lax.axis_size("sp")
    top_count = routes.shape[1]
    model_width = normed.shape[1]
    capacity = max(2, 2 * tok_dev * top_count // (columns * experts_n))
    slot_total = experts_n * capacity
    own_routes = lax.dynamic_slice_in_dim(routes, column * rows_own, rows_own, 0)
    own_weights = lax.dynamic_slice_in_dim(route_weights, column * rows_own, rows_own, 0)
    own_slots = slot_numbers(own_routes, capacity, experts_n)
    routing_table = dispatch_matrix(own_slots, slot_total)
    outgoing = jnp.dot(routing_table, normed, preferred_element_type=jnp.float32).astype(
        jnp.bfloat16
    )
    outgoing = outgoing.reshape(experts_n, capacity, model_width)
    arrived = lax.all_to_all(outgoing, "sp", split_axis=0, concat_axis=1, tiled=True).reshape(
        slot_total, model_width
    )
    gate_act = jnp.dot(arrived, whole_gate, preferred_element_type=jnp.float32)
    up_act = jnp.dot(arrived, whole_up, preferred_element_type=jnp.float32)
    hidden = (jax.nn.silu(gate_act) * up_act).astype(jnp.bfloat16)
    summed = jnp.dot(hidden, whole_down, preferred_element_type=jnp.float32)
    expert_out = summed.astype(jnp.bfloat16).reshape(experts_n, capacity, model_width)
    returned = lax.all_to_all(expert_out, "sp", split_axis=0, concat_axis=0, tiled=True).reshape(
        slot_total, model_width
    )
    combined = stream
    for member in range(top_count):
        chosen = jnp.take(returned, own_slots[:, member], axis=0).astype(jnp.float32)
        combined = combined + own_weights[:, member : member + 1] * chosen
    return combined.astype(jnp.bfloat16)


def solution(mesh):
    return jax.shard_map(
        shards,
        mesh=mesh,
        in_specs=(
            P(("sp", "tp"), None),
            P("sp", "tp"),
            P("sp", "tp"),
            P("sp"),
            P(None, "tp"),
            P("tp"),
            P("tp"),
            P(),
            P(),
            P("sp", None),
            P("sp", None),
            P("sp", None, "tp"),
            P("sp", None, "tp"),
            P("sp", "tp", None),
        ),
        out_specs=P(("sp", "tp"), None),
        check_vma=False,
    )
```

profile of v0, /device:TPU:0, one launch (start us, length us, event | category | flops | bytes accessed | tf_op | source)
XLA Modules:
  0.0 198.8 jit_solution(16494497963675948296)
XLA Ops:
  6.5 0.0 copy-start
  6.5 0.0 copy-start.5
  6.5 0.0 all-gather.7.cloned.1.call-start
  6.6 0.7 all-gather.7.cloned.1.call-update
  7.3 0.0 all-gather.11.cloned.1.call-start
  7.3 0.7 all-gather.11.cloned.1.call-update
  8.0 0.0 all-gather.9.cloned.1.call-start
  8.1 0.0 copy-done.5
  8.1 0.1 slice.300
  8.2 4.9 %collective-permute-start = (s32[30]{0:T(128)S(1)}, s32[30]{0:T(128)S(1)}, u32[]{:S(2)}, u32[]{:S(2)}) collective-permute-start(s32[30]{0:T(128)S(1)} %slice.300), channel_id=1, source_target_pairs={{0,4},{4,8},{8,12},{12,16},{16,20},{20,24},{24,28},{1,5},{5,9},{9,... | collective-permute-start | bytes 368 | tf_op jit(solution)/shard_map/ppermute | solution.py:13
  13.0 0.0 copy-done.3
  13.0 0.0 copy-done.2
  13.0 0.2 multiply_convert_fusion.4
  13.2 3.5 %collective-permute-start.1 = (bf16[30,256]{1,0:T(8,128)(2,1)S(1)}, bf16[30,256]{1,0:T(8,128)(2,1)S(1)}, u32[]{:S(2)}, u32[]{:S(2)}) collective-permute-start(bf16[30,256]{1,0:T(8,128)(2,1)S(1)} %slice.404), channel_id=1, source_target_pairs={{0,4},{4,8},{8,12},{12,16},{16,20},{20,24},{24,28},{1,5},{5,9},{9,... | collective-permute-start | bytes 46088 | tf_op jit(solution)/shard_map/ppermute | solution.py:13
  16.7 0.0 all-gather.9.cloned.1.call-update
  16.7 0.0 copy-done.4
  16.8 0.0 copy-done
  16.8 0.1 copy.22
  16.9 0.1 eq.163
  17.1 0.1 eq.159
  17.2 0.6 reduce-window.6
  17.8 0.2 slice_reduce_fusion.2
  18.1 0.1 fusion.79
  18.1 0.1 reduce_sum.41
  18.3 0.0 collective-permute-done
  18.3 0.1 pad_add_fusion
  18.4 0.1 slice_compare_fusion.29
  18.5 0.1 slice_compare_fusion.28
  18.6 0.0 collective-permute-done.1
  18.6 0.1 maximum_convert_fusion
  18.6 4.0 %fusion.15 = f32[512,256]{1,0:T(8,128)S(1)} fusion(f32[542,256]{1,0:T(8,128)S(1)} %maximum_convert_fusion, f32[256]{0:T(256)S(1)} %bitcast.154, f32[256]{0:T(256)S(1)} %bitcast.156, f32[256]{0:T(256)S(1)} %bitcast.98, f32[256]{0:T(256)S(1)} %bitcast.100, f32[256]{0:T(256)S(1)} %bitcast.102, f32[256]{0:T(256)S(1)} %bitcast.104, f32[256]{0:T(256)S(1)} %bitcast.106, ...), kind=kLoop, calls=%fused_computation.21 | loop fusion | flops 11927552 | bytes 16824320 | tf_op jit(solution)/shard_map/add | solution.py:63
  22.7 0.3 reshape.109
  23.0 0.0 copy-start.7
  23.0 0.0 copy-start.8
  23.0 0.6 reduce_sum.38
  23.6 1.6 multiply_reduce_fusion.1
  25.3 0.6 mul.492
  25.9 0.6 sub.20
  26.5 0.0 copy-done.7
  26.5 0.0 copy-done.8
  26.5 5.0 %multiply_convert_fusion.3 = bf16[512,256]{1,0:T(8,128)(2,1)} fusion(f32[64,8,2,128]{3,2,1,0:T(2,128)S(1)} %bitcast.89, f32[64,8,2,128]{3,2,1,0:T(2,128)S(1)} %bitcast.90, f32[256]{0:T(256)S(1)} %copy-done.7, f32[256]{0:T(256)S(1)} %copy-done.8, f32[256]{0:T(256)S(1)} %bitcast.155, f32[542,256]{1,0:T(8,128)S(1)} %maximum_convert_fusion, ...), kind=kLoop, calls=%fused_computation.114 | loop fusion | flops 13107200 | bytes 17612800 | tf_op jit(solution)/shard_map/convert_element_type | solution.py:73
  31.5 3.4 %all-to-all-start = ((bf16[4,128,256]{2,1,0:T(8,128)(2,1)}), bf16[4,128,256]{2,1,0:T(8,128)(2,1)S(1)}, u32[]{:S(2)}, u32[]{:S(2)}) async-start(bf16[4,128,256]{2,1,0:T(8,128)(2,1)} %bitcast.31), calls=%async_computation | async-start | bytes 524288 | tf_op jit(solution)/shard_map/all_to_all | solution.py:77
  34.9 0.1 copy.21
  35.0 0.1 fusion.77
  35.1 9.0 %all-to-all-done = bf16[4,128,256]{2,1,0:T(8,128)(2,1)S(1)} async-done(((bf16[4,128,256]{2,1,0:T(8,128)(2,1)}), bf16[4,128,256]{2,1,0:T(8,128)(2,1)S(1)}, u32[]{:S(2)}, u32[]{:S(2)}) %all-to-all-start) | async-done | bytes 262176 | tf_op jit(solution)/shard_map/all_to_all | solution.py:77
  44.1 0.2 copy.19
  44.3 0.0 copy-start.1
  44.3 0.0 copy-start.6
  44.3 3.0 %convolution_convert_fusion.1 = bf16[128,2048]{1,0:T(8,128)(2,1)S(1)} fusion(bf16[128,1024]{0,1:T(8,128)(2,1)S(1)} %bitcast.94, bf16[1024,2048]{1,0:T(8,128)(2,1)} %param.23), kind=kOutput, calls=%fused_computation.10 | convolution fusion | flops 537133056 | bytes 4980736 | tf_op jit(solution)/shard_map/dot_general | solution.py:78
  47.3 0.0 copy-done.1
  47.3 0.3 multiply_reduce_fusion
  47.6 0.0 copy-done.6
  47.6 0.8 convolution_convert_fusion
  48.4 54.0 %all_to_all.33 = bf16[8,64,2048]{2,1,0:T(8,128)(2,1)S(1)} all-to-all(bf16[8,64,2048]{2,1,0:T(8,128)(2,1)S(1)} %bitcast.88), channel_id=1, replica_groups=mesh['sp'=8,'tp'=4] {'sp'}, dimensions={0} | all-to-all | bytes 4194304 | tf_op jit(solution)/shard_map/all_to_all | solution.py:98
  102.4 5.9 %fusion.4 = f32[512,1024]{1,0:T(8,128)} fusion(bf16[512,2048]{1,0:T(8,128)(2,1)S(1)} %bitcast.92, bf16[1,2048,1024]{2,1,0:T(8,128)(2,1)} %all-gather.7.cloned.1.call-done), kind=kOutput, calls=%fused_computation.6 | convolution fusion | flops 2147483648 | bytes 8388608 | tf_op jit(solution)/shard_map/dot_general | solution.py:101
  108.3 13.8 %all-gather.9.cloned.1.call-done = bf16[1,2048,1024]{2,1,0:T(8,128)(2,1)} async-done(((bf16[1,2048,256]{2,1,0:T(8,128)(2,1)}), bf16[1,2048,1024]{2,1,0:T(8,128)(2,1)}) %all-gather.9.cloned.1.call-update) | async-done | bytes 4194320 | tf_op jit(solution)/shard_map/all_gather | solution.py:49
  122.1 10.0 %fusion.6 = bf16[512,2048]{1,0:T(8,128)(2,1)} fusion(bf16[1,1024,2048]{2,1,0:T(8,128)(2,1)} %all-gather.11.cloned.1.call-done, f32[512,1024]{1,0:T(8,128)} %fusion.4, bf16[512,2048]{1,0:T(8,128)(2,1)S(1)} %bitcast.93, bf16[1,2048,1024]{2,1,0:T(8,128)(2,1)} %all-gather.9.cloned.1.call-done), kind=kOutput, calls=%fused_computation.8 | convolution fusion | flops 4299161600 | bytes 14680064 | tf_op jit(solution)/shard_map/dot_general | solution.py:104
  132.2 5.5 %all-to-all-start.2 = ((bf16[8,64,2048]{2,1,0:T(8,128)(2,1)}), bf16[8,64,2048]{2,1,0:T(8,128)(2,1)S(1)}, u32[]{:S(2)}, u32[]{:S(2)}) async-start(bf16[8,64,2048]{2,1,0:T(8,128)(2,1)} %bitcast.91), calls=%async_computation.2 | async-start | bytes 4194304 | tf_op jit(solution)/shard_map/all_to_all | solution.py:106
  137.7 0.7 constant_dynamic-slice_fusion.1
  138.3 0.2 slice_reduce_fusion.1
  138.6 47.7 %all-to-all-done.2 = bf16[8,64,2048]{2,1,0:T(8,128)(2,1)S(1)} async-done(((bf16[8,64,2048]{2,1,0:T(8,128)(2,1)}), bf16[8,64,2048]{2,1,0:T(8,128)(2,1)S(1)}, u32[]{:S(2)}, u32[]{:S(2)}) %all-to-all-start.2) | async-done | bytes 2097184 | tf_op jit(solution)/shard_map/all_to_all | solution.py:106
  186.3 1.7 gather_fusion
  188.0 1.7 gather_fusion.1
  189.8 2.5 %add_convert_fusion = bf16[128,2048]{1,0:T(8,128)(2,1)} fusion(bf16[128,2048]{1,0:T(8,128)(2,1)S(1)} %convolution_convert_fusion.1, bf16[128,2048]{1,0:T(8,128)(2,1)S(1)} %copy-done.1, bf16[128,2048]{1,0:T(8,128)(2,1)} %gather_fusion.1, bf16[128,2048]{1,0:T(8,128)(2,1)} %gather_fusion, f32[128]{0:T(128)S(1)} %get-tuple-element.70, ...), kind=kLoop, calls=%fused_computation.12 | loop fusion | flops 3145728 | bytes 2622720 | tf_op jit(solution)/shard_map/convert_element_type | solution.py:113
  (21 shorter events, 0.2 us)
Async XLA Ops:
  6.5 10.2 %copy-start = (s32[512,2]{0,1:T(2,128)S(1)}, s32[512,2]{0,1:T(2,128)}, u32[]{:S(2)}) copy-start(s32[512,2]{0,1:T(2,128)} %param.25) | copy-start | bytes 12292
  6.5 1.5 copy-start.5
  6.5 6.5 %copy-start.3 = (bf16[512,256]{1,0:T(8,128)(2,1)S(1)}, bf16[512,256]{1,0:T(8,128)(2,1)}, u32[]{:S(2)}) copy-start(bf16[512,256]{1,0:T(8,128)(2,1)} %param.17) | copy-start | bytes 786436
  6.5 6.5 %copy-start.2 = (bf16[512,256]{1,0:T(8,128)(2,1)S(1)}, bf16[512,256]{1,0:T(8,128)(2,1)}, u32[]{:S(2)}) copy-start(bf16[512,256]{1,0:T(8,128)(2,1)} %param.18) | copy-start | bytes 786436
  6.5 10.2 %copy-start.4 = (f32[31,256]{1,0:T(8,128)S(1)}, f32[31,256]{1,0:T(8,128)}, u32[]{:S(2)}) copy-start(f32[31,256]{1,0:T(8,128)} %param.20) | copy-start | bytes 95236
  6.5 95.9 %all-gather.7.cloned.1.call-start = ((), (), s32[]{:S(2)}) async-start(), calls=%async_computation.3 | async-start | bytes 5242880 | tf_op jit(solution)/shard_map/all_gather | solution.py:48
  7.3 101.0 %all-gather.11.cloned.1.call-start = ((), (), s32[]{:S(2)}) async-start(), calls=%async_computation.5 | async-start | bytes 5242880 | tf_op jit(solution)/shard_map/all_gather | solution.py:51
  8.0 114.1 %all-gather.9.cloned.1.call-start = ((), (), s32[]{:S(2)}) async-start(), calls=%async_computation.4 | async-start | bytes 5242880 | tf_op jit(solution)/shard_map/all_gather | solution.py:49
  8.2 10.1 %collective-permute-start = (s32[30]{0:T(128)S(1)}, s32[30]{0:T(128)S(1)}, u32[]{:S(2)}, u32[]{:S(2)}) collective-permute-start(s32[30]{0:T(128)S(1)} %slice.300), channel_id=1, source_target_pairs={{0,4},{4,8},{8,12},{12,16},{16,20},{20,24},{24,28},{1,5},{5,9},{9,... | collective-permute-start | bytes 368 | tf_op jit(solution)/shard_map/ppermute | solution.py:13
  13.2 5.4 %collective-permute-start.1 = (bf16[30,256]{1,0:T(8,128)(2,1)S(1)}, bf16[30,256]{1,0:T(8,128)(2,1)S(1)}, u32[]{:S(2)}, u32[]{:S(2)}) collective-permute-start(bf16[30,256]{1,0:T(8,128)(2,1)S(1)} %slice.404), channel_id=1, source_target_pairs={{0,4},{4,8},{8,12},{12,16},{16,20},{20,24},{24,28},{1,5},{5,9},{9,... | collective-permute-start | bytes 46088 | tf_op jit(solution)/shard_map/ppermute | solution.py:13
  23.0 3.5 %copy-start.7 = (f32[256]{0:T(256)S(1)}, f32[256]{0:T(256)}, u32[]{:S(2)}) copy-start(f32[256]{0:T(256)} %param.22) | copy-start | bytes 3076
  23.0 3.5 %copy-start.8 = (f32[256]{0:T(256)S(1)}, f32[256]{0:T(256)}, u32[]{:S(2)}) copy-start(f32[256]{0:T(256)} %param.21) | copy-start | bytes 3076
  31.5 12.6 %all-to-all-start = ((bf16[4,128,256]{2,1,0:T(8,128)(2,1)}), bf16[4,128,256]{2,1,0:T(8,128)(2,1)S(1)}, u32[]{:S(2)}, u32[]{:S(2)}) async-start(bf16[4,128,256]{2,1,0:T(8,128)(2,1)} %bitcast.31), calls=%async_computation | async-start | bytes 524288 | tf_op jit(solution)/shard_map/all_to_all | solution.py:77
  44.3 3.0 %copy-start.1 = (bf16[128,2048]{1,0:T(8,128)(2,1)S(1)}, bf16[128,2048]{1,0:T(8,128)(2,1)}, u32[]{:S(2)}) copy-start(bf16[128,2048]{1,0:T(8,128)(2,1)} %param.16) | copy-start | bytes 1572868
  44.3 3.3 %copy-start.6 = (f32[2048]{0:T(1024)S(1)}, f32[2048]{0:T(1024)}, u32[]{:S(2)}) copy-start(f32[2048]{0:T(1024)} %param.24) | copy-start | bytes 24580
  132.2 54.2 %all-to-all-start.2 = ((bf16[8,64,2048]{2,1,0:T(8,128)(2,1)}), bf16[8,64,2048]{2,1,0:T(8,128)(2,1)S(1)}, u32[]{:S(2)}, u32[]{:S(2)}) async-start(bf16[8,64,2048]{2,1,0:T(8,128)(2,1)} %bitcast.91), calls=%async_computation.2 | async-start | bytes 4194304 | tf_op jit(solution)/shard_map/all_to_all | solution.py:106
Sparse Core Ops, SparseCore 0:
  8.9 40.5 all-gather.6
  51.0 34.4 all-gather.10
  87.1 34.9 all-gather.8
where the time goes:
time: 199 us
  waiting for transfers between devices  72 us (36%)
  blocking collectives  54 us (27%)
  matrix products  19.7 us (10%)
  starting transfers between devices  17.3 us (9%)
  other arithmetic  15.3 us (8%)
  between operations  13.5 us (7%)
  local copies, waits for them, and re-layouts  6.92 us (3%)
    all_to_all x1, blocking collectives, shards(): lax.all_to_all(outgoing, 'sp', split_axis=0, concat_axis=1, tiled=True)  54 us
    all_to_all x1, waiting for transfers between devices, shards(): lax.all_to_all(expert_out, 'sp', split_axis=0, concat_axis=0, tiled=True)  47.7 us
    all_gather x1, waiting for transfers between devices, shards(): lax.all_gather(w_up[0], 'tp', axis=1, tiled=True)  13.8 us
    dot_general x1, matrix products, shards(): summed = jnp.dot(hidden, whole_down, preferred_element_type=jnp.float32)  10 us
    all_to_all x1, waiting for transfers between devices, shards(): lax.all_to_all(conv_out, 'tp', split_axis=0, concat_axis=1, tiled=True)  9.03 us
    ppermute x2, starting transfers between devices, passed_along(): lax.ppermute(value, axis, [(source, source + steps) for source in range(i...  8.32 us
    dot_general x1, matrix products, shards(): gate_act = jnp.dot(arrived, whole_gate, preferred_element_type=jnp.float32)  5.89 us
    all_to_all x1, starting transfers between devices, shards(): lax.all_to_all(expert_out, 'sp', split_axis=0, concat_axis=0, tiled=True)  5.51 us
  transfers between devices with their start and end apart: 7, of which 3 were waited for; matrix products, arithmetic and copies ran while one was open for 13% of the time, Pallas kernels for 0%

commit v1 on v0

--- a/solution.py
+++ b/solution.py
@@ -74,7 +74,10 @@
     columns = lax.axis_size("tp")
     column = lax.axis_index("tp")
     rows_own = tok_dev // columns
-    own_conv = lax.all_to_all(conv_out, "tp", split_axis=0, concat_axis=1, tiled=True)
+    own_conv = jnp.concatenate(
+        lax.all_to_all(jnp.stack(jnp.split(conv_out, lax.axis_size("tp"), axis=0)), "tp", 0, 0),
+        axis=1,
+    )
     mixed = jnp.dot(own_conv, out_weight, preferred_element_type=jnp.float32)
     stream = residual.astype(jnp.float32) + lax.optimization_barrier(
         mixed.astype(jnp.bfloat16)

time: 199 us -> 199 us (level)
  waiting for transfers between devices: 72 us -> 76.5 us
  other arithmetic: 15.3 us -> 11.5 us
    reduce_sum x1, other arithmetic: 0.61 us -> 6.28 us  [shards(): group_mean = jnp.mean(grouped, axis=-1, keepdims=True)]
    convert_element_type x1, other arithmetic: 4.99 us -> 0.25 us  [shards(): conv_out = jax.nn.silu(scaled).astype(jnp.bfloat16)]
    all_gather x1, waiting for transfers between devices: 13.8 us -> 18.3 us  [shards(): lax.all_gather(w_up[0], 'tp', axis=1, tiled=True)]
    add x1 -> x0, other arithmetic: 4.03 us -> none  [shards(): convolved + jnp.where(same_doc, extended[offset:offset + tok_dev] * conv_...]
  transfers between devices with their start and end apart: 7 -> 7, of which waited for: 3 -> 3; matrix products, arithmetic and copies ran while one was open for 13% -> 11% of each run, Pallas kernels for 0% -> 0%
where the time goes in v1:
time: 199 us
  waiting for transfers between devices  76.5 us (38%)
  blocking collectives  54.5 us (27%)
  matrix products  19.8 us (10%)
  starting transfers between devices  17.3 us (9%)
  between operations  13.5 us (7%)
  other arithmetic  11.5 us (6%)
  local copies, waits for them, and re-layouts  5.69 us (3%)
    all_to_all x1, blocking collectives, shards(): lax.all_to_all(outgoing, 'sp', split_axis=0, concat_axis=1, tiled=True)  54.5 us
    all_to_all x1, waiting for transfers between devices, shards(): lax.all_to_all(expert_out, 'sp', split_axis=0, concat_axis=0, tiled=True)  47.7 us
    all_gather x1, waiting for transfers between devices, shards(): lax.all_gather(w_up[0], 'tp', axis=1, tiled=True)  18.3 us
    dot_general x1, matrix products, shards(): summed = jnp.dot(hidden, whole_down, preferred_element_type=jnp.float32)  10 us
    all_to_all x1, waiting for transfers between devices, shards(): lax.all_to_all(jnp.stack(jnp.split(conv_out, lax.axis_size('tp'), axis=0)...  9.04 us
    ppermute x2, starting transfers between devices, passed_along(): lax.ppermute(value, axis, [(source, source + steps) for source in range(i...  8.32 us
    reduce_sum x1, other arithmetic, shards(): group_mean = jnp.mean(grouped, axis=-1, keepdims=True)  6.28 us
    dot_general x1, matrix products, shards(): gate_act = jnp.dot(arrived, whole_gate, preferred_element_type=jnp.float32)  5.98 us
  transfers between devices with their start and end apart: 7, of which 3 were waited for; matrix products, arithmetic and copies ran while one was open for 11% of the time, Pallas kernels for 0%

profile of v1, /device:TPU:0, one launch (start us, length us, event | category | flops | bytes accessed | tf_op | source)
XLA Modules:
  0.0 198.8 jit_solution(11046535242621036208)
XLA Ops:
  6.5 0.0 copy-start
  6.5 0.0 copy-start.5
  6.5 0.0 copy-start.2
  6.5 0.0 copy-start.3
  6.5 0.0 all-gather.7.cloned.1.call-start
  6.6 0.7 all-gather.7.cloned.1.call-update
  7.3 0.0 copy-start.4
  7.3 0.0 all-gather.11.cloned.1.call-start
  7.3 0.7 all-gather.11.cloned.1.call-update
  8.0 0.0 all-gather.9.cloned.1.call-start
  8.1 0.0 copy-done.5
  8.1 0.1 slice.300
  8.2 4.9 %collective-permute-start = (s32[30]{0:T(128)S(1)}, s32[30]{0:T(128)S(1)}, u32[]{:S(2)}, u32[]{:S(2)}) collective-permute-start(s32[30]{0:T(128)S(1)} %slice.300), channel_id=1, source_target_pairs={{0,4},{4,8},{8,12},{12,16},{16,20},{20,24},{24,28},{1,5},{5,9},{9,... | collective-permute-start | bytes 368 | tf_op jit(solution)/shard_map/ppermute | solution.py:13
  13.0 0.0 copy-done.2
  13.0 0.1 copy.22
  13.2 0.0 copy-done.3
  13.2 0.1 copy.23
  13.3 0.1 multiply_convert_fusion.4
  13.5 0.1 slice.404
  13.6 3.5 %collective-permute-start.1 = (bf16[30,256]{0,1:T(8,128)(2,1)S(1)}, bf16[30,256]{0,1:T(8,128)(2,1)S(1)}, u32[]{:S(2)}, u32[]{:S(2)}) collective-permute-start(bf16[30,256]{0,1:T(8,128)(2,1)S(1)} %slice.404), channel_id=1, source_target_pairs={{0,4},{4,8},{8,12},{12,16},{16,20},{20,24},{24,28},{1,5},{5,9},{9,... | collective-permute-start | bytes 46088 | tf_op jit(solution)/shard_map/ppermute | solution.py:13
  17.1 0.0 all-gather.9.cloned.1.call-update
  17.1 0.0 copy-done.4
  17.1 0.0 copy-done
  17.2 0.1 copy.26
  17.3 0.1 eq.163
  17.4 0.1 eq.159
  17.6 0.6 reduce-window.6
  18.2 0.2 slice_reduce_fusion.2
  18.4 0.1 fusion.81
  18.5 0.1 reduce_sum.41
  18.7 0.0 collective-permute-done
  18.7 0.1 pad_add_fusion
  18.8 0.1 slice_compare_fusion.29
  18.9 0.1 slice_compare_fusion.28
  18.9 0.0 collective-permute-done.1
  19.0 0.2 maximum_convert_fusion
  19.1 0.0 copy-start.7
  19.1 0.0 copy-start.8
  19.1 6.3 %bitcast_reduce_fusion = (f32[512,2]{0,1:T(2,128)S(1)}, f32[512,256]{0,1:T(8,128)S(1)}) fusion(f32[256]{0:T(256)S(1)} %bitcast.135, f32[542,256]{0,1:T(8,128)S(1)} %maximum_convert_fusion, f32[256]{0:T(256)S(1)} %bitcast.136, pred[512]{0:T(512)(128)(4,1)S(1)} %get-tuple-element.73, f32[256]{0:T(256)S(1)} %bitcast.107, ...), kind=kLoop, calls=%fused_computation.112 | loop fusion | flops 12057600 | bytes 16828416 | tf_op jit(solution)/shard_map/reduce_sum | solution.py:68
  25.4 0.1 fusion.76
  25.5 0.0 copy-done.7
  25.5 0.0 copy-done.8
  25.6 0.2 multiply_convert_fusion.3
  25.9 0.7 pad_maximum_fusion
  26.6 3.4 %all-to-all-start = ((bf16[4,128,256]{1,2,0:T(8,128)(2,1)}), bf16[4,128,256]{1,2,0:T(8,128)(2,1)S(1)}, u32[]{:S(2)}, u32[]{:S(2)}) async-start(bf16[4,128,256]{1,2,0:T(8,128)(2,1)} %pad_maximum_fusion), calls=%async_computation | async-start | bytes 524288 | tf_op jit(solution)/shard_map/all_to_all | solution.py:78
  30.0 0.1 copy.25
  30.1 0.1 fusion.79
  30.2 9.0 %all-to-all-done = bf16[4,128,256]{1,2,0:T(8,128)(2,1)S(1)} async-done(((bf16[4,128,256]{1,2,0:T(8,128)(2,1)}), bf16[4,128,256]{1,2,0:T(8,128)(2,1)S(1)}, u32[]{:S(2)}, u32[]{:S(2)}) %all-to-all-start) | async-done | bytes 262176 | tf_op jit(solution)/shard_map/all_to_all | solution.py:78
  39.2 3.0 %convolution_convert_fusion.1 = bf16[128,2048]{1,0:T(8,128)(2,1)S(1)} fusion(bf16[128,1024]{0,1:T(8,128)(2,1)S(1)} %bitcast.105, bf16[1024,2048]{1,0:T(8,128)(2,1)} %param.23), kind=kOutput, calls=%fused_computation.10 | convolution fusion | flops 537133056 | bytes 4980736 | tf_op jit(solution)/shard_map/dot_general | solution.py:81
  42.2 0.0 copy-done.1
  42.2 0.3 multiply_reduce_fusion
  42.5 0.0 copy-done.6
  42.5 0.8 convolution_convert_fusion
  43.3 54.5 %all_to_all.19 = bf16[8,64,2048]{2,1,0:T(8,128)(2,1)S(1)} all-to-all(bf16[8,64,2048]{2,1,0:T(8,128)(2,1)S(1)} %bitcast.101), channel_id=1, replica_groups=mesh['sp'=8,'tp'=4] {'sp'}, dimensions={0} | all-to-all | bytes 4194304 | tf_op jit(solution)/shard_map/all_to_all | solution.py:101
  97.8 6.0 %fusion.4 = f32[512,1024]{1,0:T(8,128)} fusion(bf16[512,2048]{1,0:T(8,128)(2,1)S(1)} %bitcast.103, bf16[1,2048,1024]{2,1,0:T(8,128)(2,1)} %all-gather.7.cloned.1.call-done), kind=kOutput, calls=%fused_computation.6 | convolution fusion | flops 2147483648 | bytes 8388608 | tf_op jit(solution)/shard_map/dot_general | solution.py:104
  103.8 18.3 %all-gather.9.cloned.1.call-done = bf16[1,2048,1024]{2,1,0:T(8,128)(2,1)} async-done(((bf16[1,2048,256]{2,1,0:T(8,128)(2,1)}), bf16[1,2048,1024]{2,1,0:T(8,128)(2,1)}) %all-gather.9.cloned.1.call-update) | async-done | bytes 4194320 | tf_op jit(solution)/shard_map/all_gather | solution.py:49
  122.1 10.0 %fusion.6 = bf16[512,2048]{1,0:T(8,128)(2,1)} fusion(bf16[1,1024,2048]{2,1,0:T(8,128)(2,1)} %all-gather.11.cloned.1.call-done, f32[512,1024]{1,0:T(8,128)} %fusion.4, bf16[512,2048]{1,0:T(8,128)(2,1)S(1)} %bitcast.104, bf16[1,2048,1024]{2,1,0:T(8,128)(2,1)} %all-gather.9.cloned.1.call-done), kind=kOutput, calls=%fused_computation.8 | convolution fusion | flops 4299161600 | bytes 14680064 | tf_op jit(solution)/shard_map/dot_general | solution.py:107
  132.1 5.5 %all-to-all-start.2 = ((bf16[8,64,2048]{2,1,0:T(8,128)(2,1)}), bf16[8,64,2048]{2,1,0:T(8,128)(2,1)S(1)}, u32[]{:S(2)}, u32[]{:S(2)}) async-start(bf16[8,64,2048]{2,1,0:T(8,128)(2,1)} %bitcast.102), calls=%async_computation.2 | async-start | bytes 4194304 | tf_op jit(solution)/shard_map/all_to_all | solution.py:109
  137.6 0.7 constant_dynamic-slice_fusion.1
  138.3 0.2 slice_reduce_fusion.1
  138.5 47.7 %all-to-all-done.2 = bf16[8,64,2048]{2,1,0:T(8,128)(2,1)S(1)} async-done(((bf16[8,64,2048]{2,1,0:T(8,128)(2,1)}), bf16[8,64,2048]{2,1,0:T(8,128)(2,1)S(1)}, u32[]{:S(2)}, u32[]{:S(2)}) %all-to-all-start.2) | async-done | bytes 2097184 | tf_op jit(solution)/shard_map/all_to_all | solution.py:109
  186.3 1.7 gather_fusion
  188.0 1.7 gather_fusion.1
  189.7 2.5 %add_convert_fusion = bf16[128,2048]{1,0:T(8,128)(2,1)} fusion(bf16[128,2048]{1,0:T(8,128)(2,1)S(1)} %convolution_convert_fusion.1, bf16[128,2048]{1,0:T(8,128)(2,1)S(1)} %copy-done.1, bf16[128,2048]{1,0:T(8,128)(2,1)} %gather_fusion.1, bf16[128,2048]{1,0:T(8,128)(2,1)} %gather_fusion, f32[128]{0:T(128)S(1)} %get-tuple-element.76, ...), kind=kLoop, calls=%fused_computation.12 | loop fusion | flops 3145728 | bytes 2622720 | tf_op jit(solution)/shard_map/convert_element_type | solution.py:116
  (20 shorter events, 0.2 us)
Async XLA Ops:
  6.5 10.6 %copy-start = (s32[512,2]{0,1:T(2,128)S(1)}, s32[512,2]{0,1:T(2,128)}, u32[]{:S(2)}) copy-start(s32[512,2]{0,1:T(2,128)} %param.25) | copy-start | bytes 12292
  6.5 1.5 copy-start.5
  6.5 6.5 %copy-start.2 = (bf16[512,256]{1,0:T(8,128)(2,1)S(1)}, bf16[512,256]{1,0:T(8,128)(2,1)}, u32[]{:S(2)}) copy-start(bf16[512,256]{1,0:T(8,128)(2,1)} %param.17) | copy-start | bytes 786436
  6.5 6.6 %copy-start.3 = (bf16[512,256]{1,0:T(8,128)(2,1)S(1)}, bf16[512,256]{1,0:T(8,128)(2,1)}, u32[]{:S(2)}) copy-start(bf16[512,256]{1,0:T(8,128)(2,1)} %param.18) | copy-start | bytes 786436
  6.5 91.3 %all-gather.7.cloned.1.call-start = ((), (), s32[]{:S(2)}) async-start(), calls=%async_computation.3 | async-start | bytes 5242880 | tf_op jit(solution)/shard_map/all_gather | solution.py:48
  7.3 9.8 %copy-start.4 = (f32[31,256]{1,0:T(8,128)S(1)}, f32[31,256]{1,0:T(8,128)}, u32[]{:S(2)}) copy-start(f32[31,256]{1,0:T(8,128)} %param.20) | copy-start | bytes 95236
  7.3 96.5 %all-gather.11.cloned.1.call-start = ((), (), s32[]{:S(2)}) async-start(), calls=%async_computation.5 | async-start | bytes 5242880 | tf_op jit(solution)/shard_map/all_gather | solution.py:51
  8.0 114.1 %all-gather.9.cloned.1.call-start = ((), (), s32[]{:S(2)}) async-start(), calls=%async_computation.4 | async-start | bytes 5242880 | tf_op jit(solution)/shard_map/all_gather | solution.py:49
  8.2 10.5 %collective-permute-start = (s32[30]{0:T(128)S(1)}, s32[30]{0:T(128)S(1)}, u32[]{:S(2)}, u32[]{:S(2)}) collective-permute-start(s32[30]{0:T(128)S(1)} %slice.300), channel_id=1, source_target_pairs={{0,4},{4,8},{8,12},{12,16},{16,20},{20,24},{24,28},{1,5},{5,9},{9,... | collective-permute-start | bytes 368 | tf_op jit(solution)/shard_map/ppermute | solution.py:13
  13.6 5.4 %collective-permute-start.1 = (bf16[30,256]{0,1:T(8,128)(2,1)S(1)}, bf16[30,256]{0,1:T(8,128)(2,1)S(1)}, u32[]{:S(2)}, u32[]{:S(2)}) collective-permute-start(bf16[30,256]{0,1:T(8,128)(2,1)S(1)} %slice.404), channel_id=1, source_target_pairs={{0,4},{4,8},{8,12},{12,16},{16,20},{20,24},{24,28},{1,5},{5,9},{9,... | collective-permute-start | bytes 46088 | tf_op jit(solution)/shard_map/ppermute | solution.py:13
  19.1 6.4 %copy-start.7 = (f32[256]{0:T(256)S(1)}, f32[256]{0:T(256)}, u32[]{:S(2)}) copy-start(f32[256]{0:T(256)} %param.22) | copy-start | bytes 3076
  19.1 6.4 %copy-start.8 = (f32[256]{0:T(256)S(1)}, f32[256]{0:T(256)}, u32[]{:S(2)}) copy-start(f32[256]{0:T(256)} %param.21) | copy-start | bytes 3076
  26.6 12.6 %all-to-all-start = ((bf16[4,128,256]{1,2,0:T(8,128)(2,1)}), bf16[4,128,256]{1,2,0:T(8,128)(2,1)S(1)}, u32[]{:S(2)}, u32[]{:S(2)}) async-start(bf16[4,128,256]{1,2,0:T(8,128)(2,1)} %pad_maximum_fusion), calls=%async_computation | async-start | bytes 524288 | tf_op jit(solution)/shard_map/all_to_all | solution.py:78
  39.2 3.0 %copy-start.1 = (bf16[128,2048]{1,0:T(8,128)(2,1)S(1)}, bf16[128,2048]{1,0:T(8,128)(2,1)}, u32[]{:S(2)}) copy-start(bf16[128,2048]{1,0:T(8,128)(2,1)} %param.16) | copy-start | bytes 1572868
  39.2 3.3 %copy-start.6 = (f32[2048]{0:T(1024)S(1)}, f32[2048]{0:T(1024)}, u32[]{:S(2)}) copy-start(f32[2048]{0:T(1024)} %param.24) | copy-start | bytes 24580
  132.1 54.2 %all-to-all-start.2 = ((bf16[8,64,2048]{2,1,0:T(8,128)(2,1)}), bf16[8,64,2048]{2,1,0:T(8,128)(2,1)S(1)}, u32[]{:S(2)}, u32[]{:S(2)}) async-start(bf16[8,64,2048]{2,1,0:T(8,128)(2,1)} %bitcast.102), calls=%async_computation.2 | async-start | bytes 4194304 | tf_op jit(solution)/shard_map/all_to_all | solution.py:109
Sparse Core Ops, SparseCore 0:
  8.9 40.5 all-gather.6
  51.0 34.4 all-gather.10
  87.1 34.9 all-gather.8
